TPU v7x, 32 devices: a whole 2x2x4 slice. The times are simulated.
32 devices in a mesh: gr: 2 (over y), sp: 4 (over z), tp: 4 (over x, core).
Axes of the slice: x: 2, y: 2, z: 4, core: 2. Of those that a mesh axis runs over, the one named last changes fastest.
Arguments:
- tokens: bfloat16 [8, 768, 4096], P('gr', 'sp'), parts along dimension 0, may hold values from -50 to 50
- new_tokens: bfloat16 [8, 4096], P('gr'), parts along dimension 0, may hold values from -6 to 6
- in_gain: float32 [4096], replicated, may hold values from 0.1 to 1.9
- w_forget: bfloat16 [4096, 2048], P(None, 'tp'), may hold values from -0.09375 to 0.09375
- w_value: bfloat16 [4096, 2048], P(None, 'tp'), may hold values from -0.75 to 0.75
- gap: float32 [16, 128], P('tp'), may hold values from 0 to 0.06
- decay_shift: float32 [8, 768, 16], P('gr', 'sp', 'tp'), parts along dimension 0, may hold values from -3 to 0
- query: bfloat16 [8, 16, 128], P('gr', 'tp', 'sp'), parts along dimension 0, may hold values from -6 to 6
- out_gain: float32 [16, 128], P('tp'), may hold values from 0.1 to 1.9
Outputs:
- cache: bfloat16 [8, 16, 128, 128], P('gr', 'tp', 'sp'), parts along dimension 0
- read: float32 [8, 16, 128], P('gr', 'tp'), parts along dimension 0
There are 2 independent parts, one for each index of `gr`. A program takes and returns all parts, laid end to end along the dimension named above; an argument that names none is the same for every part. Nothing has to cross between parts.
All inputs are finite; a program needn't handle non-finite values.
Results may differ from a plain program's by a relative error of at most 0.0065.
Values sent between devices are 32-bit elements; how exact they have to be, the bound alone decides.
A program may use at most 64 MiB of HBM per device.

v0:
```python
import jax
import jax.numpy as jnp
from jax import lax
from jax.sharding import PartitionSpec as P

epsilon = 1e-06


def normalize(row_block, gain_row):
    widened = row_block.astype(jnp.float32)
    scaled = widened * lax.rsqrt(jnp.mean(widened * widened, axis=-1, keepdims=True) + epsilon)
    return (scaled * gain_row).astype(jnp.bfloat16)


def settle(received):
    stacked, block_sums = received
    later_sum = jnp.cumsum(block_sums[::-1], axis=0)[::-1] - block_sums
    return jnp.sum(jnp.exp(later_sum)[..., None] * stacked, axis=0)


def local(tokens, new_tokens, in_gain, w_forget, w_value, gap, decay_shift, query, out_gain):
    seq_count, seg_len, model_width = tokens.shape
    head_count, key_dim = gap.shape
    val_dim = out_gain.shape[1]
    row_count = key_dim // lax.axis_size("sp")
    unit_norm_rows = normalize(tokens.reshape(seq_count * seg_len, model_width), in_gain)
    forget_pre = jnp.dot(unit_norm_rows, w_forget, preferred_element_type=jnp.float32).reshape(
        seq_count, seg_len, head_count, key_dim
    )
    values = jnp.dot(unit_norm_rows, w_value, preferred_element_type=jnp.float32).astype(
        jnp.bfloat16
    )
    values = values.reshape(seq_count, seg_len, head_count, val_dim)
    key_gate = gap * jax.nn.sigmoid(-forget_pre)
    forget_logarithm = jnp.log1p(-key_gate) + decay_shift[:, :, :, None]
    totals = jnp.sum(forget_logarithm, axis=1)
    within = totals[:, None] - jnp.cumsum(forget_logarithm, axis=1)
    weights = (key_gate * jnp.exp(within)).astype(jnp.bfloat16)
    pieces = jnp.einsum("sthi,sthj->shij", weights, values, preferred_element_type=jnp.float32)
    full_state = settle(
        (
            lax.all_to_all(pieces[None], "sp", split_axis=3, concat_axis=0, tiled=True),
            lax.all_to_all(totals[None], "sp", split_axis=3, concat_axis=0, tiled=True),
        )
    )
    cache = full_state.astype(jnp.bfloat16)
    row_start = lax.axis_index("sp") * row_count
    normed_new = normalize(new_tokens, in_gain)
    new_pre = jnp.dot(normed_new, w_forget, preferred_element_type=jnp.float32).reshape(
        seq_count, head_count, key_dim
    )
    new_key = lax.dynamic_slice_in_dim(gap * jax.nn.sigmoid(-new_pre), row_start, row_count, 2)
    new_values = lax.optimization_barrier(
        jnp.dot(normed_new, w_value, preferred_element_type=jnp.float32).astype(jnp.bfloat16)
    )
    new_values = new_values.astype(jnp.float32).reshape(seq_count, head_count, val_dim)
    updated = (1.0 - new_key)[..., None] * full_state + new_key[..., None] * new_values[
        :, :, None, :
    ]
    partial_value = jnp.einsum(
        "shi,shij->shj", query.astype(jnp.float32), updated, precision=lax.Precision.HIGHEST
    )
    read_raw = lax.psum(partial_value, "sp")
    read = (
        read_raw
        * lax.rsqrt(jnp.mean(read_raw * read_raw, axis=-1, keepdims=True) + epsilon)
        * out_gain
    )
    return (cache, read)


def solution(mesh):
    return jax.shard_map(
        local,
        mesh=mesh,
        in_specs=(
            P("gr", "sp", None),
            P("gr", None),
            P(),
            P(None, "tp"),
            P(None, "tp"),
            P("tp", None),
            P("gr", "sp", "tp"),
            P("gr", "tp", "sp"),
            P("tp", None),
        ),
        out_specs=(P("gr", "tp", "sp", None), P("gr", "tp", None)),
        check_vma=False,
    )
```

profile of v0, /device:TPU:0, one launch (start us, length us, event | category | flops | bytes accessed | tf_op | source)
XLA Modules:
  0.0 92.6 jit_solution(18022183195930927783)
XLA Ops:
  0.7 6.4 %copy.34 = bf16[512,4096]{1,0:T(8,128)(2,1)} copy(bf16[512,4096]{0,1:T(8,128)(2,1)} %bitcast.65) | data formatting | bytes 8388608 | tf_op jit(solution)/shard_map/dot_general | solution.py:27
  7.1 4.2 %multiply_reduce_fusion = f32[4,192]{1,0:T(4,128)S(1)} fusion(bf16[4,192,4096]{2,1,0:T(8,128)(2,1)} %param.9), kind=kLoop, calls=%fused_computation.4 | loop fusion | flops 9436416 | bytes 6294528 | tf_op jit(solution)/shard_map/reduce_sum | solution.py:11
  11.7 6.4 %fusion.15 = (f32[4,128,4,192]{1,3,2,0:T(8,128)S(1)}, f32[4,192,4,128]{3,1,2,0:T(8,128)S(1)}) fusion(f32[4,4,192]{2,1,0:T(4,128)S(1)} %bitcast.79, f32[128,4]{0,1:T(4,128)S(1)} %bitcast.78, bf16[4,128,4096,1]{2,1,0,3:T(8,128)(2,1)} %bitcast.70, f32[4096]{0:T(1024)S(1)} %copy-done.6, f32[4,192]{1,0:T(4,128)S(1)} %add_rsqrt_fusion, ...), kind=kOutput, calls=%fused_computation.19 | convolution fusion | flops 3235774464 | bytes 13665280 | tf_op jit(solution)/shard_map/dot_general | solution.py:27
  18.1 1.1 %copy-done.4 = f32[4,192,4,128]{3,1,2,0:T(8,128)} copy-done((f32[4,192,4,128]{3,1,2,0:T(8,128)}, f32[4,192,4,128]{3,1,2,0:T(8,128)S(1)}, u32[]{:S(2)}) %copy-start.4) | copy-done | bytes 1572888
  19.3 0.7 add_reduce_fusion
  20.2 0.9 reshape.91
  21.0 6.3 %all-to-all-start = ((f32[4,1,512]{2,1,0:T(1,128)}), f32[4,1,512]{2,1,0:T(1,128)S(1)}, u32[]{:S(2)}, u32[]{:S(2)}) async-start(f32[4,1,512]{2,1,0:T(1,128)} %reshape.91), calls=%async_computation | async-start | bytes 16384 | tf_op jit(solution)/shard_map/all_to_all | solution.py:43
  27.7 1.6 %fusion.8 = f32[4,128,4,2,128]{1,3,2,4,0:T(2,128)S(1)} fusion(f32[4,128,4,2,128]{1,4,3,2,0:T(8,128)S(1)} %bitcast.68), kind=kOutput, calls=%fused_computation.10 | output fusion | flops 66584576 | bytes 4194304 | tf_op jit(solution)/shard_map/reduce-window
  29.3 1.3 %copy-done.2 = f32[4,128,4,2,128]{1,3,2,4,0:T(2,128)} copy-done((f32[4,128,4,2,128]{1,3,2,4,0:T(2,128)}, f32[4,128,4,2,128]{1,3,2,4,0:T(2,128)S(1)}, u32[]{:S(2)}) %copy-start.2) | copy-done | bytes 2097176
  30.8 1.9 %broadcast_add_fusion = f32[4,128,1,8,128]{1,3,2,4,0:T(8,128)S(1)} fusion(f32[4,128,1,8,128]{1,3,2,4,0:T(8,128)} %bitcast.66, f32[4,128,1,8]{1,3,2,0:T(8,128)S(1)} %bitcast.76), kind=kLoop, calls=%fused_computation.29 | loop fusion | flops 524288 | bytes 4210688 | tf_op jit(solution)/shard_map/reduce_window_sum
  32.6 1.7 %copy.24 = f32[4,128,4,2,128]{1,4,3,2,0:T(8,128)} copy(f32[4,128,4,2,128]{1,3,2,4,0:T(2,128)S(1)} %bitcast.67) | data formatting | bytes 4194304 | tf_op jit(solution)/shard_map/reduce_window_sum
  34.4 2.7 %fusion.1 = bf16[768,4096]{1,0:T(8,128)(2,1)S(1)} fusion(f32[4096]{0:T(1024)S(1)} %copy-done.6, f32[768]{0:T(1024)S(1)} %rsqrt.29, bf16[4,192,4096]{2,1,0:T(8,128)(2,1)S(1)} %bitcast.64), kind=kLoop, calls=%fused_computation.2 | loop fusion | flops 12582912 | bytes 12602368 | tf_op jit(solution)/shard_map/convert_element_type | solution.py:12
  37.1 6.6 %convolution_convert_fusion = bf16[768,512]{1,0:T(8,128)(2,1)} fusion(bf16[768,4096]{1,0:T(8,128)(2,1)S(1)} %fusion.1, bf16[4096,512]{1,0:T(8,128)(2,1)} %param.13), kind=kOutput, calls=%fused_computation.22 | convolution fusion | flops 3221618688 | bytes 11272192 | tf_op jit(solution)/shard_map/dot_general | solution.py:30
  43.8 1.7 %reshape.84 = bf16[4,192,4,128]{3,2,1,0:T(4,128)(2,1)S(1)} reshape(bf16[768,512]{1,0:T(8,128)(2,1)} %convolution_convert_fusion) | data formatting | bytes 1572864 | tf_op jit(solution)/shard_map/reshape | solution.py:33
  45.5 2.1 %convolution_bitcast_fusion = f32[1,4,4,128,128]{4,3,2,1,0:T(8,128)S(1)} fusion(f32[4,256,4,128]{3,1,2,0:T(8,128)S(1)} %bitcast.69, f32[4,192,4,128]{3,1,2,0:T(8,128)} %copy-done.4, bf16[4,192,4,128]{3,2,1,0:T(4,128)(2,1)S(1)} %reshape.84, f32[4,4,128]{2,1,0:T(4,128)S(1)} %add_reduce_fusion, f32[4,128]{1,0:T(4,128)S(1)} %copy-done.7), kind=kOutput, calls=%fused_computation.23 | convolution fusion | flops 102236160 | bytes 4990976 | tf_op jit(solution)/shard_map/sthi,sthj->shij/dot_general | solution.py:39
  47.8 1.7 %copy.26 = f32[1,4,4,128,128]{4,2,1,0,3:T(4,128)} copy(f32[1,4,4,128,128]{4,3,2,1,0:T(8,128)S(1)} %convolution_bitcast_fusion) | data formatting | bytes 2097152 | tf_op jit(solution)/shard_map/broadcast_in_dim | solution.py:42
  49.5 5.1 %all-to-all-start.1 = ((f32[1,4,4,128,128]{4,2,1,0,3:T(4,128)}), f32[1,4,4,128,128]{4,2,1,0,3:T(4,128)S(1)}, u32[]{:S(2)}, u32[]{:S(2)}) async-start(f32[1,4,4,128,128]{4,2,1,0,3:T(4,128)} %copy.26), calls=%async_computation.1 | async-start | bytes 2097152 | tf_op jit(solution)/shard_map/all_to_all | solution.py:42
  54.6 2.9 %convolution_convert_fusion.1 = bf16[4,512]{1,0:T(4,128)(2,1)S(1)} fusion(bf16[4096,512]{1,0:T(8,128)(2,1)} %param.13, bf16[4,4096]{1,0:T(4,128)(2,1)S(1)} %copy-done.5, f32[4096]{0:T(1024)S(1)} %copy-done.6, f32[4]{0:T(128)S(1)} %add_rsqrt_fusion.2), kind=kOutput, calls=%fused_computation.27 | convolution fusion | flops 16844800 | bytes 4247568 | tf_op jit(solution)/shard_map/dot_general | solution.py:54
  57.5 2.9 %fusion.19 = f32[4,512]{1,0:T(4,128)S(1)} fusion(bf16[4096,512]{1,0:T(8,128)(2,1)} %param.12, bf16[4,4096]{1,0:T(4,128)(2,1)S(1)} %copy-done.5, f32[4096]{0:T(1024)S(1)} %copy-done.6, f32[4]{0:T(128)S(1)} %add_rsqrt_fusion.2), kind=kOutput, calls=%fused_computation.26 | convolution fusion | flops 16846848 | bytes 4251664 | tf_op jit(solution)/shard_map/dot_general | solution.py:49
  62.5 17.2 %all-to-all-done.1 = f32[1,4,4,128,128]{4,2,1,0,3:T(4,128)S(1)} async-done(((f32[1,4,4,128,128]{4,2,1,0,3:T(4,128)}), f32[1,4,4,128,128]{4,2,1,0,3:T(4,128)S(1)}, u32[]{:S(2)}, u32[]{:S(2)}) %all-to-all-start.1) | async-done | bytes 1048608 | tf_op jit(solution)/shard_map/all_to_all | solution.py:42
  79.7 0.8 multiply_reduce_fusion.1
  80.8 0.7 copy.29
  81.8 10.0 %psum.7 = f32[4,4,128]{2,1,0:T(4,128)S(1)} all-reduce(f32[4,4,128]{2,1,0:T(4,128)S(1)} %bitcast.77), channel_id=1, replica_groups=mesh['gr'=2,'sp'=4,'tp'=4] {'sp'}, use_global_device_ids=true, to_apply=%region_7.8 | all-reduce | flops 2048 | bytes 16384 | tf_op jit(solution)/shard_map/psum | solution.py:63
  91.9 0.7 multiply_multiply_fusion
  (49 shorter events, 3.9 us)
Async XLA Ops:
  0.6 80.9 %copy-start = (bf16[4,4,32]{2,1,0:T(4,128)(2,1)S(1)}, bf16[4,4,32]{2,1,0:T(4,128)(2,1)}, u32[]{:S(2)}) copy-start(bf16[4,4,32]{2,1,0:T(4,128)(2,1)} %param.16) | copy-start | bytes 3076
  0.6 10.7 %copy-start.7 = (f32[4,128]{1,0:T(4,128)S(1)}, f32[4,128]{1,0:T(4,128)}, u32[]{:S(2)}) copy-start(f32[4,128]{1,0:T(4,128)} %param.14) | copy-start | bytes 6148
  0.7 10.7 %copy-start.8 = (f32[4,192,4]{1,2,0:T(4,128)S(1)}, f32[4,192,4]{1,2,0:T(4,128)}, u32[]{:S(2)}) copy-start(f32[4,192,4]{1,2,0:T(4,128)} %param.15) | copy-start | bytes 36868
  7.1 4.6 %copy-start.1 = (bf16[4,192,4096]{2,1,0:T(8,128)(2,1)S(1)}, bf16[4,192,4096]{2,1,0:T(8,128)(2,1)}, u32[]{:S(2)}) copy-start(bf16[4,192,4096]{2,1,0:T(8,128)(2,1)} %param.9) | copy-start | bytes 18874372
  7.1 4.6 %copy-start.6 = (f32[4096]{0:T(1024)S(1)}, f32[4096]{0:T(1024)}, u32[]{:S(2)}) copy-start(f32[4096]{0:T(1024)} %param.11) | copy-start | bytes 49156
  18.1 1.2 %copy-start.4 = (f32[4,192,4,128]{3,1,2,0:T(8,128)}, f32[4,192,4,128]{3,1,2,0:T(8,128)S(1)}, u32[]{:S(2)}) copy-start(f32[4,192,4,128]{3,1,2,0:T(8,128)S(1)} %get-tuple-element.9) | copy-start | bytes 4718596
  21.0 28.4 %all-to-all-start = ((f32[4,1,512]{2,1,0:T(1,128)}), f32[4,1,512]{2,1,0:T(1,128)S(1)}, u32[]{:S(2)}, u32[]{:S(2)}) async-start(f32[4,1,512]{2,1,0:T(1,128)} %reshape.91), calls=%async_computation | async-start | bytes 16384 | tf_op jit(solution)/shard_map/all_to_all | solution.py:43
  27.7 6.7 %slice-start = ((s8[6291456]{0:T(1024)(128)(4,1)}), s8[2097152]{0:T(1024)(128)(4,1)S(1)}, s32[]{:S(2)}) async-start(s8[6291456]{0:T(1024)(128)(4,1)} %bitcast.63), calls=%async_computation.2 | async-start | bytes 4194304
  29.3 1.4 %copy-start.2 = (f32[4,128,4,2,128]{1,3,2,4,0:T(2,128)}, f32[4,128,4,2,128]{1,3,2,4,0:T(2,128)S(1)}, u32[]{:S(2)}) copy-start(f32[4,128,4,2,128]{1,3,2,4,0:T(2,128)S(1)} %fusion.8) | copy-start | bytes 6291460
  30.7 3.6 %slice-start.1 = ((s8[6291456]{0:T(1024)(128)(4,1)}), s8[4194304]{0:T(1024)(128)(4,1)S(1)}, s32[]{:S(2)}) async-start(s8[6291456]{0:T(1024)(128)(4,1)} %bitcast.63), calls=%async_computation.3 | async-start | bytes 8388608
  37.1 8.4 %copy-start.3 = (f32[4,128,4,2,128]{1,4,3,2,0:T(8,128)S(1)}, f32[4,128,4,2,128]{1,4,3,2,0:T(8,128)}, u32[]{:S(2)}) copy-start(f32[4,128,4,2,128]{1,4,3,2,0:T(8,128)} %copy.24) | copy-start | bytes 6291460
  45.5 2.1 %copy-start.5 = (bf16[4,4096]{1,0:T(4,128)(2,1)S(1)}, bf16[4,4096]{1,0:T(4,128)(2,1)}, u32[]{:S(2)}) copy-start(bf16[4,4096]{1,0:T(4,128)(2,1)} %param.10) | copy-start | bytes 98308
  49.5 30.3 %all-to-all-start.1 = ((f32[1,4,4,128,128]{4,2,1,0,3:T(4,128)}), f32[1,4,4,128,128]{4,2,1,0,3:T(4,128)S(1)}, u32[]{:S(2)}, u32[]{:S(2)}) async-start(f32[1,4,4,128,128]{4,2,1,0,3:T(4,128)} %copy.26), calls=%async_computation.1 | async-start | bytes 2097152 | tf_op jit(solution)/shard_map/all_to_all | solution.py:42
  62.3 29.6 %copy-start.9 = (f32[4,128]{1,0:T(4,128)S(1)}, f32[4,128]{1,0:T(4,128)}, u32[]{:S(2)}) copy-start(f32[4,128]{1,0:T(4,128)} %param.17) | copy-start | bytes 6148
where the time goes:
time: 93.1 us; the launch traced here: 92.6 us
  matrix products  21.2 us (23%)
  local copies, waits for them, and re-layouts  17.7 us (19%)
  waiting for transfers between devices  17.2 us (18%)
  other arithmetic  14.2 us (15%)
  starting transfers between devices  11.4 us (12%)
  blocking collectives  9.98 us (11%)
    all_to_all x1, waiting for transfers between devices, local(): lax.all_to_all(pieces[None], 'sp', split_axis=3, concat_axis=0, tiled=True)  17.2 us
    psum x1, blocking collectives, local(): read_raw = lax.psum(partial_value, 'sp')  9.98 us
    dot_general x1, matrix products, local(): jnp.dot(unit_norm_rows, w_value, preferred_element_type=jnp.float32)  6.62 us
    dot_general x1, local copies, waits for them, and re-layouts, local(): jnp.dot(unit_norm_rows, w_forget, preferred_element_type=jnp.float32)  6.42 us
    dot_general x1, matrix products, local(): jnp.dot(unit_norm_rows, w_forget, preferred_element_type=jnp.float32)  6.41 us
    all_to_all x1, starting transfers between devices, local(): lax.all_to_all(totals[None], 'sp', split_axis=3, concat_axis=0, tiled=True)  6.35 us
    all_to_all x1, starting transfers between devices, local(): lax.all_to_all(pieces[None], 'sp', split_axis=3, concat_axis=0, tiled=True)  5.1 us
    unnamed x27, local copies, waits for them, and re-layouts  4.8 us
  transfers between devices with their start and end apart: 2, of which 1 were waited for; matrix products, arithmetic and copies ran while one was open for 31% of the time, Pallas kernels for 0%

commit v1 on v0

--- a/solution.py
+++ b/solution.py
@@ -60,7 +60,10 @@
     partial_value = jnp.einsum(
         "shi,shij->shj", query.astype(jnp.float32), updated, precision=lax.Precision.HIGHEST
     )
-    read_raw = lax.psum(partial_value, "sp")
+    size, read_raw = (lax.axis_size("sp"), partial_value)
+    for far in [1 << k for k in range(size.bit_length() - 1)]:
+        swap = [(i, i ^ far) for i in range(size)]
+        read_raw = read_raw + lax.ppermute(read_raw, "sp", swap)
     read = (
         read_raw
         * lax.rsqrt(jnp.mean(read_raw * read_raw, axis=-1, keepdims=True) + epsilon)

time: 93.1 us -> 90.7 us (0.974)
  blocking collectives: 9.98 us -> 0 us
  waiting for transfers between devices: 17.2 us -> 24.7 us
    psum x1 -> x0, blocking collectives: 9.98 us -> none  [local(): read_raw = lax.psum(partial_value, 'sp')]
    ppermute x0 -> x2, waiting for transfers between devices: none -> 7.49 us  [local(): read_raw = read_raw + lax.ppermute(read_raw, 'sp', swap)]
  transfers between devices with their start and end apart: 2 -> 4, of which waited for: 1 -> 3; matrix products, arithmetic and copies ran while one was open for 31% -> 32% of each run, Pallas kernels for 0% -> 0%
where the time goes in v1:
time: 90.7 us; the launch traced here: 90.2 us
  waiting for transfers between devices  24.7 us (27%)
  matrix products  21.2 us (23%)
  local copies, waits for them, and re-layouts  17.7 us (20%)
  other arithmetic  14.2 us (16%)
  starting transfers between devices  11.5 us (13%)
    all_to_all x1, waiting for transfers between devices, local(): lax.all_to_all(pieces[None], 'sp', split_axis=3, concat_axis=0, tiled=True)  17.2 us
    ppermute x2, waiting for transfers between devices, local(): read_raw = read_raw + lax.ppermute(read_raw, 'sp', swap)  7.49 us
    dot_general x1, matrix products, local(): jnp.dot(unit_norm_rows, w_value, preferred_element_type=jnp.float32)  6.62 us
    dot_general x1, local copies, waits for them, and re-layouts, local(): jnp.dot(unit_norm_rows, w_forget, preferred_element_type=jnp.float32)  6.42 us
    dot_general x1, matrix products, local(): jnp.dot(unit_norm_rows, w_forget, preferred_element_type=jnp.float32)  6.41 us
    all_to_all x1, starting transfers between devices, local(): lax.all_to_all(totals[None], 'sp', split_axis=3, concat_axis=0, tiled=True)  6.35 us
    all_to_all x1, starting transfers between devices, local(): lax.all_to_all(pieces[None], 'sp', split_axis=3, concat_axis=0, tiled=True)  5.1 us
    unnamed x27, local copies, waits for them, and re-layouts  4.8 us
  transfers between devices with their start and end apart: 4, of which 3 were waited for; matrix products, arithmetic and copies ran while one was open for 32% of the time, Pallas kernels for 0%

profile of v1, /device:TPU:0, one launch (start us, length us, event | category | flops | bytes accessed | tf_op | source)
XLA Modules:
  0.0 90.2 jit_solution(6845965586532249835)
XLA Ops:
  0.7 6.4 %copy.34 = bf16[512,4096]{1,0:T(8,128)(2,1)} copy(bf16[512,4096]{0,1:T(8,128)(2,1)} %bitcast.65) | data formatting | bytes 8388608 | tf_op jit(solution)/shard_map/dot_general | solution.py:27
  7.1 4.2 %multiply_reduce_fusion = f32[4,192]{1,0:T(4,128)S(1)} fusion(bf16[4,192,4096]{2,1,0:T(8,128)(2,1)} %param.9), kind=kLoop, calls=%fused_computation.4 | loop fusion | flops 9436416 | bytes 6294528 | tf_op jit(solution)/shard_map/reduce_sum | solution.py:11
  11.7 6.4 %fusion.15 = (f32[4,128,4,192]{1,3,2,0:T(8,128)S(1)}, f32[4,192,4,128]{3,1,2,0:T(8,128)S(1)}) fusion(f32[4,4,192]{2,1,0:T(4,128)S(1)} %bitcast.80, f32[128,4]{0,1:T(4,128)S(1)} %bitcast.79, bf16[4,128,4096,1]{2,1,0,3:T(8,128)(2,1)} %bitcast.70, f32[4096]{0:T(1024)S(1)} %copy-done.6, f32[4,192]{1,0:T(4,128)S(1)} %add_rsqrt_fusion, ...), kind=kOutput, calls=%fused_computation.19 | convolution fusion | flops 3235774464 | bytes 13665280 | tf_op jit(solution)/shard_map/dot_general | solution.py:27
  18.1 1.1 %copy-done.4 = f32[4,192,4,128]{3,1,2,0:T(8,128)} copy-done((f32[4,192,4,128]{3,1,2,0:T(8,128)}, f32[4,192,4,128]{3,1,2,0:T(8,128)S(1)}, u32[]{:S(2)}) %copy-start.4) | copy-done | bytes 1572888
  19.3 0.7 add_reduce_fusion
  20.2 0.9 reshape.91
  21.0 6.3 %all-to-all-start = ((f32[4,1,512]{2,1,0:T(1,128)}), f32[4,1,512]{2,1,0:T(1,128)S(1)}, u32[]{:S(2)}, u32[]{:S(2)}) async-start(f32[4,1,512]{2,1,0:T(1,128)} %reshape.91), calls=%async_computation | async-start | bytes 16384 | tf_op jit(solution)/shard_map/all_to_all | solution.py:43
  27.7 1.6 %fusion.8 = f32[4,128,4,2,128]{1,3,2,4,0:T(2,128)S(1)} fusion(f32[4,128,4,2,128]{1,4,3,2,0:T(8,128)S(1)} %bitcast.68), kind=kOutput, calls=%fused_computation.10 | output fusion | flops 66584576 | bytes 4194304 | tf_op jit(solution)/shard_map/reduce-window
  29.3 1.3 %copy-done.2 = f32[4,128,4,2,128]{1,3,2,4,0:T(2,128)} copy-done((f32[4,128,4,2,128]{1,3,2,4,0:T(2,128)}, f32[4,128,4,2,128]{1,3,2,4,0:T(2,128)S(1)}, u32[]{:S(2)}) %copy-start.2) | copy-done | bytes 2097176
  30.8 1.9 %broadcast_add_fusion = f32[4,128,1,8,128]{1,3,2,4,0:T(8,128)S(1)} fusion(f32[4,128,1,8,128]{1,3,2,4,0:T(8,128)} %bitcast.66, f32[4,128,1,8]{1,3,2,0:T(8,128)S(1)} %bitcast.76), kind=kLoop, calls=%fused_computation.29 | loop fusion | flops 524288 | bytes 4210688 | tf_op jit(solution)/shard_map/reduce_window_sum
  32.6 1.7 %copy.24 = f32[4,128,4,2,128]{1,4,3,2,0:T(8,128)} copy(f32[4,128,4,2,128]{1,3,2,4,0:T(2,128)S(1)} %bitcast.67) | data formatting | bytes 4194304 | tf_op jit(solution)/shard_map/reduce_window_sum
  34.4 2.7 %fusion.1 = bf16[768,4096]{1,0:T(8,128)(2,1)S(1)} fusion(f32[4096]{0:T(1024)S(1)} %copy-done.6, f32[768]{0:T(1024)S(1)} %rsqrt.29, bf16[4,192,4096]{2,1,0:T(8,128)(2,1)S(1)} %bitcast.64), kind=kLoop, calls=%fused_computation.2 | loop fusion | flops 12582912 | bytes 12602368 | tf_op jit(solution)/shard_map/convert_element_type | solution.py:12
  37.1 6.6 %convolution_convert_fusion = bf16[768,512]{1,0:T(8,128)(2,1)} fusion(bf16[768,4096]{1,0:T(8,128)(2,1)S(1)} %fusion.1, bf16[4096,512]{1,0:T(8,128)(2,1)} %param.13), kind=kOutput, calls=%fused_computation.22 | convolution fusion | flops 3221618688 | bytes 11272192 | tf_op jit(solution)/shard_map/dot_general | solution.py:30
  43.8 1.7 %reshape.84 = bf16[4,192,4,128]{3,2,1,0:T(4,128)(2,1)S(1)} reshape(bf16[768,512]{1,0:T(8,128)(2,1)} %convolution_convert_fusion) | data formatting | bytes 1572864 | tf_op jit(solution)/shard_map/reshape | solution.py:33
  45.5 2.1 %convolution_bitcast_fusion = f32[1,4,4,128,128]{4,3,2,1,0:T(8,128)S(1)} fusion(f32[4,256,4,128]{3,1,2,0:T(8,128)S(1)} %bitcast.69, f32[4,192,4,128]{3,1,2,0:T(8,128)} %copy-done.4, bf16[4,192,4,128]{3,2,1,0:T(4,128)(2,1)S(1)} %reshape.84, f32[4,4,128]{2,1,0:T(4,128)S(1)} %add_reduce_fusion, f32[4,128]{1,0:T(4,128)S(1)} %copy-done.7), kind=kOutput, calls=%fused_computation.23 | convolution fusion | flops 102236160 | bytes 4990976 | tf_op jit(solution)/shard_map/sthi,sthj->shij/dot_general | solution.py:39
  47.8 1.7 %copy.26 = f32[1,4,4,128,128]{4,2,1,0,3:T(4,128)} copy(f32[1,4,4,128,128]{4,3,2,1,0:T(8,128)S(1)} %convolution_bitcast_fusion) | data formatting | bytes 2097152 | tf_op jit(solution)/shard_map/broadcast_in_dim | solution.py:42
  49.5 5.1 %all-to-all-start.1 = ((f32[1,4,4,128,128]{4,2,1,0,3:T(4,128)}), f32[1,4,4,128,128]{4,2,1,0,3:T(4,128)S(1)}, u32[]{:S(2)}, u32[]{:S(2)}) async-start(f32[1,4,4,128,128]{4,2,1,0,3:T(4,128)} %copy.26), calls=%async_computation.1 | async-start | bytes 2097152 | tf_op jit(solution)/shard_map/all_to_all | solution.py:42
  54.6 2.9 %convolution_convert_fusion.1 = bf16[4,512]{1,0:T(4,128)(2,1)S(1)} fusion(bf16[4096,512]{1,0:T(8,128)(2,1)} %param.13, bf16[4,4096]{1,0:T(4,128)(2,1)S(1)} %copy-done.5, f32[4096]{0:T(1024)S(1)} %copy-done.6, f32[4]{0:T(128)S(1)} %add_rsqrt_fusion.2), kind=kOutput, calls=%fused_computation.27 | convolution fusion | flops 16844800 | bytes 4247568 | tf_op jit(solution)/shard_map/dot_general | solution.py:54
  57.5 2.9 %fusion.19 = f32[4,512]{1,0:T(4,128)S(1)} fusion(bf16[4096,512]{1,0:T(8,128)(2,1)} %param.12, bf16[4,4096]{1,0:T(4,128)(2,1)S(1)} %copy-done.5, f32[4096]{0:T(1024)S(1)} %copy-done.6, f32[4]{0:T(128)S(1)} %add_rsqrt_fusion.2), kind=kOutput, calls=%fused_computation.26 | convolution fusion | flops 16846848 | bytes 4251664 | tf_op jit(solution)/shard_map/dot_general | solution.py:49
  62.5 17.2 %all-to-all-done.1 = f32[1,4,4,128,128]{4,2,1,0,3:T(4,128)S(1)} async-done(((f32[1,4,4,128,128]{4,2,1,0,3:T(4,128)}), f32[1,4,4,128,128]{4,2,1,0,3:T(4,128)S(1)}, u32[]{:S(2)}, u32[]{:S(2)}) %all-to-all-start.1) | async-done | bytes 1048608 | tf_op jit(solution)/shard_map/all_to_all | solution.py:42
  79.7 0.8 multiply_reduce_fusion.1
  81.2 3.6 %collective-permute-done = f32[4,4,128]{2,1,0:T(4,128)S(1)} collective-permute-done((f32[4,4,128]{2,1,0:T(4,128)S(1)}, f32[4,4,128]{2,1,0:T(4,128)S(1)}, u32[]{:S(2)}, u32[]{:S(2)}) %collective-permute-start) | collective-permute-done | bytes 8224 | tf_op jit(solution)/shard_map/ppermute | solution.py:66
  84.9 0.7 copy.29
  85.6 3.9 %collective-permute-done.1 = f32[4,4,128]{2,1,0:T(4,128)S(1)} collective-permute-done((f32[4,4,128]{2,1,0:T(4,128)S(1)}, f32[4,4,128]{2,1,0:T(4,128)S(1)}, u32[]{:S(2)}, u32[]{:S(2)}) %collective-permute-start.1) | collective-permute-done | bytes 8224 | tf_op jit(solution)/shard_map/ppermute | solution.py:66
  (53 shorter events, 4.7 us)
Async XLA Ops:
  0.6 80.2 %copy-start = (bf16[4,4,32]{2,1,0:T(4,128)(2,1)S(1)}, bf16[4,4,32]{2,1,0:T(4,128)(2,1)}, u32[]{:S(2)}) copy-start(bf16[4,4,32]{2,1,0:T(4,128)(2,1)} %param.16) | copy-start | bytes 3076
  0.6 10.7 %copy-start.7 = (f32[4,128]{1,0:T(4,128)S(1)}, f32[4,128]{1,0:T(4,128)}, u32[]{:S(2)}) copy-start(f32[4,128]{1,0:T(4,128)} %param.14) | copy-start | bytes 6148
  0.7 10.7 %copy-start.8 = (f32[4,192,4]{1,2,0:T(4,128)S(1)}, f32[4,192,4]{1,2,0:T(4,128)}, u32[]{:S(2)}) copy-start(f32[4,192,4]{1,2,0:T(4,128)} %param.15) | copy-start | bytes 36868
  7.1 4.6 %copy-start.1 = (bf16[4,192,4096]{2,1,0:T(8,128)(2,1)S(1)}, bf16[4,192,4096]{2,1,0:T(8,128)(2,1)}, u32[]{:S(2)}) copy-start(bf16[4,192,4096]{2,1,0:T(8,128)(2,1)} %param.9) | copy-start | bytes 18874372
  7.1 4.6 %copy-start.6 = (f32[4096]{0:T(1024)S(1)}, f32[4096]{0:T(1024)}, u32[]{:S(2)}) copy-start(f32[4096]{0:T(1024)} %param.11) | copy-start | bytes 49156
  18.1 1.2 %copy-start.4 = (f32[4,192,4,128]{3,1,2,0:T(8,128)}, f32[4,192,4,128]{3,1,2,0:T(8,128)S(1)}, u32[]{:S(2)}) copy-start(f32[4,192,4,128]{3,1,2,0:T(8,128)S(1)} %get-tuple-element.11) | copy-start | bytes 4718596
  21.0 28.4 %all-to-all-start = ((f32[4,1,512]{2,1,0:T(1,128)}), f32[4,1,512]{2,1,0:T(1,128)S(1)}, u32[]{:S(2)}, u32[]{:S(2)}) async-start(f32[4,1,512]{2,1,0:T(1,128)} %reshape.91), calls=%async_computation | async-start | bytes 16384 | tf_op jit(solution)/shard_map/all_to_all | solution.py:43
  27.7 6.7 %slice-start = ((s8[6291456]{0:T(1024)(128)(4,1)}), s8[2097152]{0:T(1024)(128)(4,1)S(1)}, s32[]{:S(2)}) async-start(s8[6291456]{0:T(1024)(128)(4,1)} %bitcast.63), calls=%async_computation.2 | async-start | bytes 4194304
  29.3 1.4 %copy-start.2 = (f32[4,128,4,2,128]{1,3,2,4,0:T(2,128)}, f32[4,128,4,2,128]{1,3,2,4,0:T(2,128)S(1)}, u32[]{:S(2)}) copy-start(f32[4,128,4,2,128]{1,3,2,4,0:T(2,128)S(1)} %fusion.8) | copy-start | bytes 6291460
  30.7 3.6 %slice-start.1 = ((s8[6291456]{0:T(1024)(128)(4,1)}), s8[4194304]{0:T(1024)(128)(4,1)S(1)}, s32[]{:S(2)}) async-start(s8[6291456]{0:T(1024)(128)(4,1)} %bitcast.63), calls=%async_computation.3 | async-start | bytes 8388608
  37.1 8.4 %copy-start.3 = (f32[4,128,4,2,128]{1,4,3,2,0:T(8,128)S(1)}, f32[4,128,4,2,128]{1,4,3,2,0:T(8,128)}, u32[]{:S(2)}) copy-start(f32[4,128,4,2,128]{1,4,3,2,0:T(8,128)} %copy.24) | copy-start | bytes 6291460
  45.5 2.1 %copy-start.5 = (bf16[4,4096]{1,0:T(4,128)(2,1)S(1)}, bf16[4,4096]{1,0:T(4,128)(2,1)}, u32[]{:S(2)}) copy-start(bf16[4,4096]{1,0:T(4,128)(2,1)} %param.10) | copy-start | bytes 98308
  49.5 30.3 %all-to-all-start.1 = ((f32[1,4,4,128,128]{4,2,1,0,3:T(4,128)}), f32[1,4,4,128,128]{4,2,1,0,3:T(4,128)S(1)}, u32[]{:S(2)}, u32[]{:S(2)}) async-start(f32[1,4,4,128,128]{4,2,1,0,3:T(4,128)} %copy.26), calls=%async_computation.1 | async-start | bytes 2097152 | tf_op jit(solution)/shard_map/all_to_all | solution.py:42
  62.3 27.2 %copy-start.9 = (f32[4,128]{1,0:T(4,128)S(1)}, f32[4,128]{1,0:T(4,128)}, u32[]{:S(2)}) copy-start(f32[4,128]{1,0:T(4,128)} %param.17) | copy-start | bytes 6148
  81.2 3.7 %collective-permute-start = (f32[4,4,128]{2,1,0:T(4,128)S(1)}, f32[4,4,128]{2,1,0:T(4,128)S(1)}, u32[]{:S(2)}, u32[]{:S(2)}) collective-permute-start(f32[4,4,128]{2,1,0:T(4,128)S(1)} %bitcast.77), channel_id=1, source_target_pairs={{0,4},{4,0},{8,12},{12,8},{1,5},{5,1},{9,13},{13,9},{2,6},{6,2},{1... | collective-permute-start | bytes 24584 | tf_op jit(solution)/shard_map/ppermute | solution.py:66
  84.9 4.5 %collective-permute-start.1 = (f32[4,4,128]{2,1,0:T(4,128)S(1)}, f32[4,4,128]{2,1,0:T(4,128)S(1)}, u32[]{:S(2)}, u32[]{:S(2)}) collective-permute-start(f32[4,4,128]{2,1,0:T(4,128)S(1)} %add.79), channel_id=1, source_target_pairs={{0,8},{4,12},{8,0},{12,4},{1,9},{5,13},{9,1},{13,5},{2,10},{6,14},... | collective-permute-start | bytes 24584 | tf_op jit(solution)/shard_map/ppermute | solution.py:66
